TPU v7x, 512 devices: a whole 4x8x8 slice. The times are simulated.
512 devices in a mesh: sp: 32 (over z, x), tp: 16 (over y, core).
Axes of the slice: x: 4, y: 8, z: 8, core: 2. Of those that a mesh axis runs over, the one named last changes fastest.
Arguments:
- queries: bfloat16 [8192, 2048], P('sp', 'tp'), may hold values from -6 to 6
- key_matrix: bfloat16 [8192, 2048], P('sp', 'tp'), may hold values from -6 to 6
- value_matrix: bfloat16 [8192, 4096], P('sp', 'tp'), may hold values from -6 to 6
- output_gate_preactivation: bfloat16 [8192, 4096], P('sp', 'tp'), may hold values from -6 to 6
- decay_preactivation: bfloat16 [8192, 2048], P('sp', 'tp')
- extra_log_decay: float32 [8192, 16], P('sp', 'tp'), may hold values from -0.7 to 0
- head_norm_gain: bfloat16 [256], replicated, may hold values from 0.099609375 to 1.8984375
- output_projection: bfloat16 [4096, 2048], P(None, 'tp'), may hold values from -0.09375 to 0.09375
- residual: bfloat16 [8192, 2048], P('sp', 'tp'), may hold values from -210 to 210
- feedforward_gain: bfloat16 [2048], replicated, may hold values from 0.099609375 to 1.8984375
- routing: int32 [8192, 4], P('sp'), may hold values from 0 to 127, all different within a row; in each aligned block of 256 rows (0 to 255, 256 to 511, ...) at most 12 rows name the same one
- router_score: float32 [8192, 4], P('sp'), may hold values from 0.05 to 1
- expert_gate_weight: bfloat16 [2048, 131072], P(None, ('sp', 'tp')), may hold values from -0.125 to 0.125
- expert_up_weight: bfloat16 [2048, 131072], P(None, ('sp', 'tp')), may hold values from -0.125 to 0.125
- expert_down_weight: bfloat16 [131072, 2048], P(('sp', 'tp')), may hold values from -0.1875 to 0.1875
- shared_expert_gate: bfloat16 [2048, 512], P(None, 'tp'), may hold values from -0.125 to 0.125
- shared_expert_up: bfloat16 [2048, 512], P(None, 'tp'), may hold values from -0.125 to 0.125
- shared_expert_down: bfloat16 [512, 2048], P(None, 'tp'), may hold values from -0.25 to 0.25
Outputs:
- layer_out: bfloat16 [8192, 2048], P('sp', 'tp')
Inputs may be any that keep to these rules, and one draw needn't show every extreme that they name: `routing`: each row names 4 different experts. In each aligned block of 256 rows, the rows of one index of sp, no expert is named by more than 12 rows, a bound that some expert reaches in some blocks.
All inputs are finite; a program needn't handle non-finite values.
Results may differ from a plain program's by a relative error of at most 0.01.
Values may be sent and summed in bfloat16 or wider, within the bound.
No kernel may reach another device: no remote copies, remote signals or barrier semaphores. Data moves between devices by JAX's collectives and lax.ppermute only.
A program may use at most 64 MiB of HBM per device.

v0:
```python
import jax
import jax.numpy as jnp
from jax import lax
from jax.sharding import Mesh
from jax.sharding import PartitionSpec as P

DK = 128
DV = 256
BLOCK_POSITIONS = 64
FF_PARTS = 4
SP = ("sp_0", "sp_1")
SP_TP = ("sp_0", "sp_1", "tp")
HIGHEST = lax.Precision.HIGHEST
EPSILON = 1e-06
ROUTE_SCALE = 2.5
GATE_TEMPER = 16.0


def nothing_yet(value, identity):
    return jax.tree.map(
        lambda part, zero: jnp.zeros_like(part) + jnp.asarray(zero, part.dtype), value, identity
    )


def prefix_by_axis(value, axes, combine, identity):
    before = start = nothing_yet(value, identity)
    total = value
    for axis in reversed(axes):
        count, position = (lax.axis_size(axis), lax.axis_index(axis))
        pieces = jax.tree.map(
            lambda part, kind: lax.all_gather(part.astype(kind), axis),
            total,
            (jnp.bfloat16, jnp.bfloat16),
        )
        inside, total = (start, start)
        for k in range(count):
            passed = k < position
            total = combine(
                total, jax.tree.map(lambda part, own: part[k].astype(own.dtype), pieces, value)
            )
            inside = jax.tree.map(lambda new, old: jnp.where(passed, new, old), total, inside)
        before = combine(inside, before)
    return before


def laid_out(blocks, dim):
    blocks = jnp.moveaxis(blocks, 0, dim)
    dims = blocks.shape
    return blocks.reshape(*dims[:dim], dims[dim] * dims[dim + 1], *dims[dim + 2 :])


def sent_to_all(value, axis):
    copies = jnp.broadcast_to(value, (lax.axis_size(axis), *value.shape))
    return lax.all_to_all(copies, axis, split_axis=0, concat_axis=0, tiled=True)


def gather_directly(value, axis, dim):
    return laid_out(sent_to_all(value, axis), dim)


def from_partner(value, axis, bit):
    mask = 2**bit
    pairs = [(source, source ^ mask) for source in range(lax.axis_size(axis))]
    return lax.ppermute(value, axis, pairs)


def carry_combine(first_part, second_part):
    return (
        first_part[0] * second_part[0],
        second_part[0][..., None] * first_part[1] + second_part[1],
    )


def attention_heads(queries, key_matrix, value_matrix, decay_preactivation, extra_log_decay):
    tokens = queries.shape[0]
    local_head_count = extra_log_decay.shape[1]
    block_count = tokens // BLOCK_POSITIONS
    query_block = queries.astype(jnp.float32).reshape(
        block_count, BLOCK_POSITIONS, local_head_count, DK
    ) * DK ** (-0.5)
    key_block = key_matrix.astype(jnp.float32).reshape(
        block_count, BLOCK_POSITIONS, local_head_count, DK
    )
    value_block = value_matrix.astype(jnp.float32).reshape(
        block_count, BLOCK_POSITIONS, local_head_count, DV
    )
    log_decay_rows = (
        jax.nn.log_sigmoid(decay_preactivation.astype(jnp.float32)).reshape(
            block_count, BLOCK_POSITIONS, local_head_count, DK
        )
        / GATE_TEMPER
    )
    log_decay_rows = (
        log_decay_rows
        + extra_log_decay.reshape(block_count, BLOCK_POSITIONS, local_head_count)[..., None]
    )
    inside = jnp.cumsum(log_decay_rows, axis=1)
    block_total = inside[:, -1]
    query_decay = query_block * jnp.exp(inside)
    key_decay = key_block * jnp.exp(-inside)
    causal = jnp.tril(jnp.ones((BLOCK_POSITIONS, BLOCK_POSITIONS), dtype=bool))
    scores = jnp.where(
        causal, jnp.einsum("nthd,nshd->nhts", query_decay, key_decay, precision=HIGHEST), 0.0
    )
    within = jnp.einsum("nhts,nshv->nthv", scores, value_block, precision=HIGHEST)
    key_end = key_block * jnp.exp(block_total[:, None] - inside)
    update = jnp.einsum("nshd,nshv->nhdv", key_end, value_block, precision=HIGHEST)
    before = jnp.cumsum(block_total, axis=0) - block_total
    ending = jnp.concatenate([before, (before[-1] + block_total[-1])[None]], axis=0)
    after_block = before + block_total
    earlier_mask = jnp.arange(block_count + 1)[:, None] > jnp.arange(block_count)[None, :]
    span_logs = jnp.where(
        earlier_mask[:, :, None, None], ending[:, None] - after_block[None], -1e30
    )
    states = jnp.einsum("nmhd,mhdv->nhdv", jnp.exp(span_logs), update, precision=HIGHEST)
    passed = jnp.einsum("nthd,nhdv->nthv", query_decay, states[:block_count], precision=HIGHEST)
    query_start = query_block * jnp.exp(inside + before[:, None])
    return (within + passed, query_start, jnp.exp(ending[block_count]), states[block_count])


def body(
    queries,
    key_matrix,
    value_matrix,
    output_gate_preactivation,
    decay_preactivation,
    extra_log_decay,
    head_norm_gain,
    output_projection,
    residual,
    feedforward_gain,
    routing,
    router_score,
    expert_gate_weight,
    expert_up_weight,
    expert_down_weight,
    shared_expert_gate,
    shared_expert_up,
    shared_expert_down,
):
    tokens = queries.shape[0]
    local_head_count = extra_log_decay.shape[1]
    local_part, query_start, dev_decay, dev_update = attention_heads(
        queries, key_matrix, value_matrix, decay_preactivation, extra_log_decay
    )
    _, entering = prefix_by_axis(
        (dev_decay, dev_update),
        SP,
        carry_combine,
        (jnp.ones_like(dev_decay), jnp.zeros_like(dev_update)),
    )
    attention_output = local_part + jnp.einsum(
        "nthd,hdv->nthv", query_start, entering, precision=HIGHEST
    )
    attention_output = attention_output.reshape(tokens, local_head_count, DV)
    inverse_rms = lax.rsqrt(
        jnp.mean(attention_output * attention_output, axis=-1, keepdims=True) + EPSILON
    )
    gate_act = jax.nn.silu(
        output_gate_preactivation.astype(jnp.float32).reshape(tokens, local_head_count, DV)
    )
    head_rows = (
        (attention_output * inverse_rms * head_norm_gain.astype(jnp.float32) * gate_act)
        .reshape(tokens, local_head_count * DV)
        .astype(jnp.bfloat16)
    )
    projected = jnp.dot(
        lax.all_gather(head_rows, "tp", axis=1, tiled=True),
        output_projection,
        preferred_element_type=jnp.float32,
    )
    mid_local = (residual.astype(jnp.float32) + projected).astype(jnp.bfloat16)
    mid_rows = gather_directly(mid_local, "tp", 1).astype(jnp.float32)
    normed = (
        mid_rows
        * lax.rsqrt(jnp.mean(mid_rows * mid_rows, axis=-1, keepdims=True) + EPSILON)
        * feedforward_gain.astype(jnp.float32)
    ).astype(jnp.bfloat16)
    shared_pre = jnp.dot(normed, shared_expert_gate, preferred_element_type=jnp.float32)
    shared_lin = jnp.dot(normed, shared_expert_up, preferred_element_type=jnp.float32)
    shared_hidden = (jax.nn.silu(shared_pre) * shared_lin).astype(jnp.bfloat16)
    senders = lax.axis_size(SP)
    tp_count = lax.axis_size("tp")
    tp_bits = tp_count.bit_length() - 1
    tp_index = lax.axis_index("tp")
    groups = tp_count // FF_PARTS
    group_here = tp_index // FF_PARTS
    part_here = tp_index % FF_PARTS
    model_width = normed.shape[1]
    picks = routing.shape[1]
    expert_total = senders * groups
    rows_most = max(2, 3 * tokens * picks // (2 * expert_total))
    slot_count = senders * rows_most
    flat_expert = routing.reshape(-1)
    one_hot = (flat_expert[:, None] == jnp.arange(expert_total, dtype=jnp.int32)[None, :]).astype(
        jnp.int32
    )
    rank_before = jnp.sum((jnp.cumsum(one_hot, axis=0) - one_hot) * one_hot, axis=1)
    owned = flat_expert % groups == group_here
    slot_index = jnp.where(owned, flat_expert // groups * rows_most + rank_before, slot_count)
    token_index = jnp.arange(flat_expert.shape[0], dtype=jnp.int32) // picks
    part_width = model_width // FF_PARTS
    normed_part = lax.dynamic_slice_in_dim(normed, part_here * part_width, part_width, 1)
    outgoing = (
        jnp.zeros((slot_count, part_width), jnp.bfloat16)
        .at[slot_index]
        .set(normed_part[token_index], mode="drop")
    )
    arrived = lax.all_to_all(
        outgoing.reshape(senders, rows_most, part_width),
        SP,
        split_axis=0,
        concat_axis=0,
        tiled=True,
    )
    for bit in range(2):
        partner_cols = from_partner(arrived, "tp", bit)
        upper = (tp_index >> bit) % 2
        arrived = jnp.where(
            upper == 1,
            jnp.concatenate([partner_cols, arrived], axis=2),
            jnp.concatenate([arrived, partner_cols], axis=2),
        )
    rows_in = arrived.reshape(slot_count, model_width)
    gate_pre = jnp.dot(rows_in, expert_gate_weight, preferred_element_type=jnp.float32)
    up_pre = jnp.dot(rows_in, expert_up_weight, preferred_element_type=jnp.float32)
    routed_hidden = (jax.nn.silu(gate_pre) * up_pre).astype(jnp.bfloat16)
    partial_out = jnp.dot(routed_hidden, expert_down_weight, preferred_element_type=jnp.float32)
    slab_width = model_width // tp_count
    partial_out = partial_out.reshape(slot_count, groups, FF_PARTS, slab_width)
    for bit in (1, 0):
        paired = partial_out.reshape(slot_count, groups, 2, 2**bit, slab_width)
        upper = (tp_index >> bit) % 2
        kept = lax.dynamic_index_in_dim(paired, upper, 2, keepdims=False)
        given = lax.dynamic_index_in_dim(paired, 1 - upper, 2, keepdims=False)
        partial_out = kept + from_partner(given.astype(jnp.bfloat16), "tp", bit).astype(given.dtype)
    expert_out = partial_out.reshape(senders, rows_most, groups, slab_width).astype(jnp.bfloat16)
    shared_out = jnp.dot(
        lax.all_gather(shared_hidden, "tp", axis=1, tiled=True),
        shared_expert_down,
        preferred_element_type=jnp.float32,
    )
    returned = lax.all_to_all(expert_out, SP, split_axis=0, concat_axis=0, tiled=True).reshape(
        slot_count, groups, slab_width
    )
    safe_slot = jnp.minimum(slot_index, slot_count - 1)
    route_weight = ROUTE_SCALE * router_score / jnp.sum(router_score, axis=1, keepdims=True)
    pair_weight = jnp.where(owned, route_weight.reshape(-1), 0.0)
    picked = returned[safe_slot].astype(jnp.float32) * pair_weight[:, None, None]
    routed_part = jnp.sum(picked.reshape(tokens, picks, groups, slab_width), axis=1)
    for bit in range(tp_bits - 1, 1, -1):
        paired = routed_part.reshape(tokens, 2, 2 ** (bit - 2), slab_width)
        upper = (tp_index >> bit) % 2
        kept = lax.dynamic_index_in_dim(paired, upper, 1, keepdims=False)
        given = lax.dynamic_index_in_dim(paired, 1 - upper, 1, keepdims=False)
        routed_part = kept + from_partner(given.astype(jnp.bfloat16), "tp", bit).astype(given.dtype)
    routed = routed_part.reshape(tokens, slab_width)
    return (mid_local.astype(jnp.float32) + routed + shared_out).astype(jnp.bfloat16)


def solution(mesh):
    finer = Mesh(mesh.devices.reshape(8, 4, mesh.shape["tp"]), ("sp_0", "sp_1", "tp"))
    in_specs = (
        P(SP, "tp"),
        P(SP, "tp"),
        P(SP, "tp"),
        P(SP, "tp"),
        P(SP, "tp"),
        P(SP, "tp"),
        P(),
        P(None, "tp"),
        P(SP, "tp"),
        P(),
        P(SP, None),
        P(SP, None),
        P(None, SP_TP),
        P(None, SP_TP),
        P(SP_TP, None),
        P(None, "tp"),
        P(None, "tp"),
        P(None, "tp"),
    )
    out_specs = P(SP, "tp")
    return jax.shard_map(body, mesh=finer, in_specs=in_specs, out_specs=out_specs, check_vma=False)
```

profile of v0, /device:TPU:1, one launch (start us, length us, event | category | flops | bytes accessed | tf_op | source)
XLA Modules:
  0.0 347.6 jit_solution(1330581877182747626)
XLA Ops:
  6.6 1.0 fusion.52
  8.1 1.3 reduce.7
  10.2 1.4 fusion.49
  11.6 1.7 convolution_bitcast_fusion
  13.6 8.5 %all_gather.22 = bf16[4,1,128]{2,1,0:T(2,128)(2,1)S(1)} all-gather(bf16[1,1,128]{2,1,0:T(2,128)(2,1)S(1)} %get-tuple-element.7), channel_id=1, replica_groups=mesh['sp_0'=8,'sp_1'=4,'tp'=16] {'sp_1'}, dimensions={0}, use_global_device_ids=true | all-gather | bytes 1280 | tf_op jit(solution)/shard_map/all_gather | solution.py:31
  22.1 18.6 %all_gather.23 = bf16[8,1,128]{2,1,0:T(2,128)(2,1)S(1)} all-gather(bf16[1,1,128]{2,1,0:T(2,128)(2,1)S(1)} %multiply_convert_fusion.1), channel_id=1, replica_groups=mesh['sp_0'=8,'sp_1'=4,'tp'=16] {'sp_0'}, dimensions={0}, use_global_device_ids=true | all-gather | bytes 2304 | tf_op jit(solution)/shard_map/all_gather | solution.py:31
  42.6 9.4 %all_gather.24 = bf16[4,1,128,256]{3,2,1,0:T(8,128)(2,1)S(1)} all-gather(bf16[1,1,128,256]{3,2,1,0:T(8,128)(2,1)S(1)} %copy.45), channel_id=1, replica_groups=mesh['sp_0'=8,'sp_1'=4,'tp'=16] {'sp_1'}, dimensions={0}, use_global_device_ids=true | all-gather | bytes 327680 | tf_op jit(solution)/shard_map/all_gather | solution.py:31
  52.6 21.8 %all_gather.25 = bf16[8,1,128,256]{3,2,1,0:T(8,128)(2,1)} all-gather(bf16[1,1,128,256]{3,2,1,0:T(8,128)(2,1)S(1)} %fusion.46), channel_id=1, replica_groups=mesh['sp_0'=8,'sp_1'=4,'tp'=16] {'sp_0'}, dimensions={0}, use_global_device_ids=true | all-gather | bytes 589824 | tf_op jit(solution)/shard_map/all_gather | solution.py:31
  75.4 1.9 multiply_reduce_fusion
  77.4 1.7 fusion.29
  79.1 53.5 %all-gather.2.cloned.1.call-done = bf16[256,4096]{1,0:T(8,128)(2,1)} async-done(((bf16[256,256]{1,0:T(8,128)(2,1)}), bf16[256,4096]{1,0:T(8,128)(2,1)}) %all-gather.2.cloned.1.call-update) | async-done | bytes 2097168 | tf_op jit(solution)/shard_map/all_gather | solution.py:168
  132.6 2.3 fusion.6
  135.5 1.2 broadcast_in_dim.52
  136.7 5.1 %all-to-all-start = ((bf16[16,256,128]{2,1,0:T(8,128)(2,1)}), bf16[16,256,128]{2,1,0:T(8,128)(2,1)S(1)}, u32[]{:S(2)}, u32[]{:S(2)}) async-start(bf16[16,256,128]{2,1,0:T(8,128)(2,1)} %broadcast_in_dim.52), calls=%async_computation | async-start | bytes 2097152 | tf_op jit(solution)/shard_map/all_to_all | solution.py:54
  143.4 26.5 %all-to-all-done = bf16[16,256,128]{2,1,0:T(8,128)(2,1)S(1)} async-done(((bf16[16,256,128]{2,1,0:T(8,128)(2,1)}), bf16[16,256,128]{2,1,0:T(8,128)(2,1)S(1)}, u32[]{:S(2)}, u32[]{:S(2)}) %all-to-all-start) | async-done | bytes 1048608 | tf_op jit(solution)/shard_map/all_to_all | solution.py:54
  170.5 9.7 %scatter_custom_fusion = bf16[384,512]{1,0:T(8,128)(2,1)S(1)} fusion(s32[1024]{0:T(1024)S(1)} %bitcast.324, bf16[256,512]{1,0:T(8,128)(2,1)S(1)} %constant_dynamic-slice_fusion.2, s32[1024]{0:T(1024)S(1)} %broadcast_clamp_fusion.1, bf16[]{:T(256)} %constant.181.clone.1), kind=kCustom, calls=%fused_computation.26 | custom fusion | bytes 393218 | tf_op jit(solution)/shard_map/scatter | solution.py:207
  180.3 27.1 %all_to_all.15 = bf16[32,12,512]{2,1,0:T(8,128)(2,1)S(1)} all-to-all(bf16[32,12,512]{2,1,0:T(8,128)(2,1)S(1)} %reshape.1386), channel_id=1, replica_groups=mesh['sp_0'=8,'sp_1'=4,'tp'=16] {'sp_0','sp_1'}, dimensions={0} | all-to-all | bytes 786432 | tf_op jit(solution)/shard_map/all_to_all | solution.py:209
  207.4 1.9 collective-permute-start
  209.3 1.9 collective-permute-done
  211.5 1.3 copy.52
  212.9 2.1 collective-permute-start.1
  215.2 1.1 maximum_select_fusion.2
  216.3 17.7 %collective-permute-done.1 = bf16[32,12,1024]{2,0,1:T(8,128)(2,1)} collective-permute-done((bf16[32,12,1024]{2,0,1:T(8,128)(2,1)}, bf16[32,12,1024]{2,0,1:T(8,128)(2,1)}, u32[]{:S(2)}, u32[]{:S(2)}) %collective-permute-start.1) | collective-permute-done | bytes 786464 | tf_op jit(solution)/shard_map/ppermute | solution.py:64
  234.0 1.6 copy.53
  235.6 1.1 concatenate.32
  236.7 2.8 fusion.18
  239.5 5.1 %fusion.19 = f32[384,2048]{1,0:T(8,128)} fusion(bf16[256,2048]{1,0:T(8,128)(2,1)S(1)} %copy-done, f32[384,256]{1,0:T(8,128)S(1)} %fusion.18, bf16[2048,256]{1,0:T(8,128)(2,1)} %param.31, bf16[384,1024]{1,0:T(8,128)(2,1)} %maximum_select_fusion.2, bf16[384,1024]{1,0:T(8,128)(2,1)S(1)} %copy-done.3, pred[]{:T(512)S(6)} %eq.66), kind=kOutput, calls=%fused_computation.48 | convolution fusion | flops 812974080 | bytes 7208961 | tf_op jit(solution)/shard_map/dot_general | solution.py:228
  244.7 5.6 %reshape_reshape.3 = f32[384,4,2,2,128]{4,3,2,1,0:T(2,128)} reshape(f32[384,2048]{1,0:T(8,128)} %fusion.19) | data formatting | bytes 6291456 | tf_op jit(solution)/shard_map/reshape;reshape | solution.py:232
  250.3 1.9 constant_dynamic-slice_fusion
  252.4 2.2 collective-permute-start.2
  254.7 2.0 constant_dynamic-slice_fusion.1
  256.6 15.9 %collective-permute-done.2 = bf16[384,4,2,128]{3,1,0,2:T(4,128)(2,1)} collective-permute-done((bf16[384,4,2,128]{3,1,0,2:T(4,128)(2,1)S(1)}, bf16[384,4,2,128]{3,1,0,2:T(4,128)(2,1)}, u32[]{:S(2)}, u32[]{:S(2)}) %collective-permute-start.2) | collective-permute-done | bytes 786464 | tf_op jit(solution)/shard_map/ppermute | solution.py:64
  272.6 1.7 bitcast_add_fusion
  274.3 1.1 copy-done.1
  275.6 3.8 %collective-permute-start.3 = (bf16[384,4,1,128]{3,1,0,2:T(4,128)(2,1)S(1)}, bf16[384,4,1,128]{3,1,0,2:T(4,128)(2,1)S(1)}, u32[]{:S(2)}, u32[]{:S(2)}) collective-permute-start(bf16[384,4,1,128]{3,1,0,2:T(4,128)(2,1)S(1)} %dynamic-slice_convert_fusion), channel_id=1, source_target_pairs={{0,1},{1,0},{2,3},{3,2},{4,5},{5,4},{6,7},{7,6},{8,9},{9,8},{10,11... | collective-permute-start | bytes 1179656 | tf_op jit(solution)/shard_map/ppermute | solution.py:64
  279.3 1.3 collective-permute-done.3
  280.6 2.1 add_convert_fusion
  282.7 4.3 %all-to-all-start.2 = ((bf16[32,12,4,128]{3,2,1,0:T(4,128)(2,1)}), bf16[32,12,4,128]{3,2,1,0:T(4,128)(2,1)S(1)}, u32[]{:S(2)}, u32[]{:S(2)}) async-start(bf16[32,12,4,128]{3,2,1,0:T(4,128)(2,1)} %bitcast.64), calls=%async_computation.2 | async-start | bytes 786432 | tf_op jit(solution)/shard_map/all_to_all | solution.py:243
  287.1 0.8 copy.56
  287.9 1.0 fusion.143
  289.0 12.0 %all-to-all-done.2 = bf16[32,12,4,128]{3,2,1,0:T(4,128)(2,1)S(1)} async-done(((bf16[32,12,4,128]{3,2,1,0:T(4,128)(2,1)}), bf16[32,12,4,128]{3,2,1,0:T(4,128)(2,1)S(1)}, u32[]{:S(2)}, u32[]{:S(2)}) %all-to-all-start.2) | async-done | bytes 393248 | tf_op jit(solution)/shard_map/all_to_all | solution.py:243
  300.9 3.6 %gather_fusion = bf16[1024,4,128]{2,1,0:T(4,128)(2,1)S(1)} fusion(bf16[384,4,128]{2,1,0:T(4,128)(2,1)S(1)} %bitcast.299, s32[1024]{0:T(1024)S(1)} %broadcast_clamp_fusion), kind=kCustom, calls=%fused_computation.1 | custom fusion | bytes 2101248 | tf_op jit(solution)/shard_map/gather | solution.py:249
  304.5 2.7 fusion.3
  307.4 4.1 %collective-permute-start.4 = (bf16[256,2,128]{2,0,1:T(8,128)(2,1)S(1)}, bf16[256,2,128]{2,0,1:T(8,128)(2,1)S(1)}, u32[]{:S(2)}, u32[]{:S(2)}) collective-permute-start(bf16[256,2,128]{2,0,1:T(8,128)(2,1)S(1)} %fusion.50), channel_id=1, source_target_pairs={{0,8},{1,9},{2,10},{3,11},{4,12},{5,13},{6,14},{7,15},{8,0},{9,1},... | collective-permute-start | bytes 393224 | tf_op jit(solution)/shard_map/ppermute | solution.py:64
  312.0 19.9 %all_gather.27 = bf16[256,512]{0,1:T(8,128)(2,1)S(1)} all-gather(bf16[256,32]{0,1:T(8,128)(2,1)S(1)} %fusion.7), channel_id=1, replica_groups=mesh['sp_0'=8,'sp_1'=4,'tp'=16] {'tp'}, dimensions={1}, use_global_device_ids=true | all-gather | bytes 278528 | tf_op jit(solution)/shard_map/all_gather | solution.py:239
  331.9 1.9 collective-permute-start.5
  334.1 6.0 %collective-permute-done.5 = bf16[256,1,128]{2,0,1:T(8,128)(2,1)S(1)} collective-permute-done((bf16[256,1,128]{2,0,1:T(8,128)(2,1)S(1)}, bf16[256,1,128]{2,0,1:T(8,128)(2,1)S(1)}, u32[]{:S(2)}, u32[]{:S(2)}) %collective-permute-start.5) | collective-permute-done | bytes 65568 | tf_op jit(solution)/shard_map/ppermute | solution.py:64
  340.1 0.7 fusion.66
  (105 shorter events, 9.7 us)
Async XLA Ops:
  6.5 233.0 %copy-start = (bf16[256,2048]{1,0:T(8,128)(2,1)S(1)}, bf16[256,2048]{1,0:T(8,128)(2,1)}, u32[]{:S(2)}) copy-start(bf16[256,2048]{1,0:T(8,128)(2,1)} %param.32) | copy-start | bytes 3145732
  6.5 126.1 %all-gather.2.cloned.1.call-start = ((), (), s32[]{:S(2)}) async-start(), calls=%async_computation.3 | async-start | bytes 2228224 | tf_op jit(solution)/shard_map/all_gather | solution.py:168
  9.9 32.0 %copy-start.12 = (bf16[256,128]{1,0:T(8,128)(2,1)S(1)}, bf16[256,128]{1,0:T(8,128)(2,1)}, u32[]{:S(2)}) copy-start(bf16[256,128]{1,0:T(8,128)(2,1)} %param.18) | copy-start | bytes 196612
  10.2 31.7 %copy-start.7 = (bf16[256,128]{1,0:T(8,128)(2,1)S(1)}, bf16[256,128]{1,0:T(8,128)(2,1)}, u32[]{:S(2)}) copy-start(bf16[256,128]{1,0:T(8,128)(2,1)} %param.19) | copy-start | bytes 196612
  11.6 30.7 %copy-start.6 = (bf16[256,256]{1,0:T(8,128)(2,1)S(1)}, bf16[256,256]{1,0:T(8,128)(2,1)}, u32[]{:S(2)}) copy-start(bf16[256,256]{1,0:T(8,128)(2,1)} %param.20) | copy-start | bytes 393220
  13.3 61.0 %copy-start.18 = (bf16[256]{0:T(256)(128)(2,1)S(1)}, bf16[256]{0:T(256)(128)(2,1)}, u32[]{:S(2)}) copy-start(bf16[256]{0:T(256)(128)(2,1)} %param.24) | copy-start | bytes 1540
  74.9 57.7 %copy-start.2 = (bf16[4096,128]{1,0:T(8,128)(2,1)S(1)}, bf16[4096,128]{1,0:T(8,128)(2,1)}, u32[]{:S(2)}) copy-start(bf16[4096,128]{1,0:T(8,128)(2,1)} %param.25) | copy-start | bytes 3145732
  75.4 2.0 copy-start.17
  75.4 57.2 %copy-start.13 = (bf16[256,128]{1,0:T(8,128)(2,1)S(1)}, bf16[256,128]{1,0:T(8,128)(2,1)}, u32[]{:S(2)}) copy-start(bf16[256,128]{1,0:T(8,128)(2,1)} %param.26) | copy-start | bytes 196612
  134.9 0.6 copy-start.4
  135.5 6.3 %copy-start.14 = (s32[256,4]{0,1:T(4,128)S(1)}, s32[256,4]{0,1:T(4,128)}, u32[]{:S(2)}) copy-start(s32[256,4]{0,1:T(4,128)} %param.28) | copy-start | bytes 12292
  135.5 6.8 %copy-start.16 = (bf16[2048]{0:T(1024)(128)(2,1)S(1)}, bf16[2048]{0:T(1024)(128)(2,1)}, u32[]{:S(2)}) copy-start(bf16[2048]{0:T(1024)(128)(2,1)} %param.27) | copy-start | bytes 12292
  136.7 33.1 %all-to-all-start = ((bf16[16,256,128]{2,1,0:T(8,128)(2,1)}), bf16[16,256,128]{2,1,0:T(8,128)(2,1)S(1)}, u32[]{:S(2)}, u32[]{:S(2)}) async-start(bf16[16,256,128]{2,1,0:T(8,128)(2,1)} %broadcast_in_dim.52), calls=%async_computation | async-start | bytes 2097152 | tf_op jit(solution)/shard_map/all_to_all | solution.py:54
  207.4 3.8 %collective-permute-start = (bf16[32,12,512]{2,1,0:T(8,128)(2,1)S(1)}, bf16[32,12,512]{2,1,0:T(8,128)(2,1)S(1)}, u32[]{:S(2)}, u32[]{:S(2)}) collective-permute-start(bf16[32,12,512]{2,1,0:T(8,128)(2,1)S(1)} %all_to_all.15), channel_id=1, source_target_pairs={{0,1},{1,0},{2,3},{3,2},{4,5},{5,4},{6,7},{7,6},{8,9},{9,8},{10,11... | collective-permute-start | bytes 1179656 | tf_op jit(solution)/shard_map/ppermute | solution.py:64
  212.9 21.2 %collective-permute-start.1 = (bf16[32,12,1024]{2,0,1:T(8,128)(2,1)}, bf16[32,12,1024]{2,0,1:T(8,128)(2,1)}, u32[]{:S(2)}, u32[]{:S(2)}) collective-permute-start(bf16[32,12,1024]{2,0,1:T(8,128)(2,1)} %copy.52), channel_id=1, source_target_pairs={{0,2},{1,3},{2,0},{3,1},{4,6},{5,7},{6,4},{7,5},{8,10},{9,11},{10,... | collective-permute-start | bytes 2359304 | tf_op jit(solution)/shard_map/ppermute | solution.py:64
  236.7 2.8 copy-start.3
  252.4 20.1 %collective-permute-start.2 = (bf16[384,4,2,128]{3,1,0,2:T(4,128)(2,1)S(1)}, bf16[384,4,2,128]{3,1,0,2:T(4,128)(2,1)}, u32[]{:S(2)}, u32[]{:S(2)}) collective-permute-start(bf16[384,4,2,128]{3,1,0,2:T(4,128)(2,1)S(1)} %bitcast.308), channel_id=1, source_target_pairs={{0,2},{1,3},{2,0},{3,1},{4,6},{5,7},{6,4},{7,5},{8,10},{9,11},{10,... | collective-permute-start | bytes 2359304 | tf_op jit(solution)/shard_map/ppermute | solution.py:64
  274.3 1.1 copy-start.1
  275.4 11.7 %copy-start.15 = (f32[256,4]{0,1:T(4,128)S(1)}, f32[256,4]{0,1:T(4,128)}, u32[]{:S(2)}) copy-start(f32[256,4]{0,1:T(4,128)} %param.29) | copy-start | bytes 12292
  275.4 12.5 %copy-start.8 = (bf16[2048,32]{0,1:T(8,128)(2,1)S(1)}, bf16[2048,32]{0,1:T(8,128)(2,1)}, u32[]{:S(2)}) copy-start(bf16[2048,32]{0,1:T(8,128)(2,1)} %param.33) | copy-start | bytes 393220
  275.6 5.1 %collective-permute-start.3 = (bf16[384,4,1,128]{3,1,0,2:T(4,128)(2,1)S(1)}, bf16[384,4,1,128]{3,1,0,2:T(4,128)(2,1)S(1)}, u32[]{:S(2)}, u32[]{:S(2)}) collective-permute-start(bf16[384,4,1,128]{3,1,0,2:T(4,128)(2,1)S(1)} %dynamic-slice_convert_fusion), channel_id=1, source_target_pairs={{0,1},{1,0},{2,3},{3,2},{4,5},{5,4},{6,7},{7,6},{8,9},{9,8},{10,11... | collective-permute-start | bytes 1179656 | tf_op jit(solution)/shard_map/ppermute | solution.py:64
  282.7 18.2 %all-to-all-start.2 = ((bf16[32,12,4,128]{3,2,1,0:T(4,128)(2,1)}), bf16[32,12,4,128]{3,2,1,0:T(4,128)(2,1)S(1)}, u32[]{:S(2)}, u32[]{:S(2)}) async-start(bf16[32,12,4,128]{3,2,1,0:T(4,128)(2,1)} %bitcast.64), calls=%async_computation.2 | async-start | bytes 786432 | tf_op jit(solution)/shard_map/all_to_all | solution.py:243
  304.5 7.0 %copy-start.9 = (bf16[2048,32]{0,1:T(8,128)(2,1)S(1)}, bf16[2048,32]{0,1:T(8,128)(2,1)}, u32[]{:S(2)}) copy-start(bf16[2048,32]{0,1:T(8,128)(2,1)} %param.34) | copy-start | bytes 393220
  304.5 7.0 %copy-start.10 = (f32[256,32]{0,1:T(8,128)S(1)}, f32[256,32]{0,1:T(8,128)}, u32[]{:S(2)}) copy-start(f32[256,32]{0,1:T(8,128)} %fusion.143) | copy-start | bytes 98308
  307.3 26.6 %copy-start.11 = (bf16[512,128]{1,0:T(8,128)(2,1)S(1)}, bf16[512,128]{1,0:T(8,128)(2,1)}, u32[]{:S(2)}) copy-start(bf16[512,128]{1,0:T(8,128)(2,1)} %param.35) | copy-start | bytes 393220
  307.3 32.8 %copy-start.5 = (bf16[256,128]{1,0:T(8,128)(2,1)S(1)}, bf16[256,128]{1,0:T(8,128)(2,1)}, u32[]{:S(2)}) copy-start(bf16[256,128]{1,0:T(8,128)(2,1)} %copy-done.4) | copy-start | bytes 196612
  307.4 24.5 %collective-permute-start.4 = (bf16[256,2,128]{2,0,1:T(8,128)(2,1)S(1)}, bf16[256,2,128]{2,0,1:T(8,128)(2,1)S(1)}, u32[]{:S(2)}, u32[]{:S(2)}) collective-permute-start(bf16[256,2,128]{2,0,1:T(8,128)(2,1)S(1)} %fusion.50), channel_id=1, source_target_pairs={{0,8},{1,9},{2,10},{3,11},{4,12},{5,13},{6,14},{7,15},{8,0},{9,1},... | collective-permute-start | bytes 393224 | tf_op jit(solution)/shard_map/ppermute | solution.py:64
  331.9 8.2 %collective-permute-start.5 = (bf16[256,1,128]{2,0,1:T(8,128)(2,1)S(1)}, bf16[256,1,128]{2,0,1:T(8,128)(2,1)S(1)}, u32[]{:S(2)}, u32[]{:S(2)}) collective-permute-start(bf16[256,1,128]{2,0,1:T(8,128)(2,1)S(1)} %dynamic-slice_convert_fusion.2), channel_id=1, source_target_pairs={{0,4},{1,5},{2,6},{3,7},{4,0},{5,1},{6,2},{7,3},{8,12},{9,13},{10,... | collective-permute-start | bytes 196616 | tf_op jit(solution)/shard_map/ppermute | solution.py:64
Sparse Core Ops, SparseCore 0:
  79.2 53.3 all-gather.1
where the time goes:
time: 349 us; the launch traced here: 348 us
  waiting for transfers between devices  135 us (39%)
  blocking collectives  105 us (30%)
  local copies, waits for them, and re-layouts  33.1 us (9%)
  starting transfers between devices  25.5 us (7%)
  matrix products  18 us (5%)
  other arithmetic  16.9 us (5%)
  between operations  14.1 us (4%)
    all_gather x4, blocking collectives, prefix_by_axis(): lax.all_gather(part.astype(kind), axis)  58.2 us
    all_gather x1, waiting for transfers between devices, body(): lax.all_gather(head_rows, 'tp', axis=1, tiled=True)  53.5 us
    ppermute x6, waiting for transfers between devices, from_partner(): return lax.ppermute(value, axis, pairs)  42.8 us
    all_to_all x1, blocking collectives, body(): lax.all_to_all(outgoing.reshape(senders, rows_most, part_width), SP, spli...  27.1 us
    all_to_all x1, waiting for transfers between devices, sent_to_all(): return lax.all_to_all(copies, axis, split_axis=0, concat_axis=0, tiled=True)  26.5 us
    all_gather x1, blocking collectives, body(): lax.all_gather(shared_hidden, 'tp', axis=1, tiled=True)  19.9 us
    ppermute x6, starting transfers between devices, from_partner(): return lax.ppermute(value, axis, pairs)  16.1 us
    all_to_all x1, waiting for transfers between devices, body(): lax.all_to_all(expert_out, SP, split_axis=0, concat_axis=0, tiled=True)  12 us
  transfers between devices with their start and end apart: 9, of which 8 were waited for; matrix products, arithmetic and copies ran while one was open for 2% of the time, Pallas kernels for 0%

commit v1 on v0

--- a/solution.py
+++ b/solution.py
@@ -14,6 +14,27 @@
 EPSILON = 1e-06
 ROUTE_SCALE = 2.5
 GATE_TEMPER = 16.0
+
+
+def ring_gather(x, axis, dim):
+    count, index, width = (lax.axis_size(axis), lax.axis_index(axis), x.shape[dim])
+    ahead = [(i, (i + 1) % count) for i in range(count)]
+    left = [(i, (i - 1) % count) for i in range(count)]
+    out = jnp.zeros((*x.shape[:dim], count * width, *x.shape[dim + 1 :]), x.dtype)
+    out = lax.dynamic_update_slice_in_dim(out, x, index * width, axis=dim)
+    from_left = from_right = x
+    halfway = count // 2
+    for step in range(1, halfway + 1):
+        from_left = lax.ppermute(from_left, axis, ahead)
+        out = lax.dynamic_update_slice_in_dim(
+            out, from_left, (index - step) % count * width, axis=dim
+        )
+        if step < count - halfway:
+            from_right = lax.ppermute(from_right, axis, left)
+            out = lax.dynamic_update_slice_in_dim(
+                out, from_right, (index + step) % count * width, axis=dim
+            )
+    return out
 
 
 def nothing_yet(value, identity):
@@ -165,9 +186,7 @@
         .astype(jnp.bfloat16)
     )
     projected = jnp.dot(
-        lax.all_gather(head_rows, "tp", axis=1, tiled=True),
-        output_projection,
-        preferred_element_type=jnp.float32,
+        ring_gather(head_rows, "tp", 1), output_projection, preferred_element_type=jnp.float32
     )
     mid_local = (residual.astype(jnp.float32) + projected).astype(jnp.bfloat16)
     mid_rows = gather_directly(mid_local, "tp", 1).astype(jnp.float32)

time: 349 us -> 330 us (0.946)
  starting transfers between devices: 25.5 us -> 72.8 us
  waiting for transfers between devices: 135 us -> 96.1 us
  between operations: 14.1 us -> 0.89 us
  blocking collectives: 105 us -> 96.7 us
    all_gather x1 -> x0, waiting for transfers between devices: 53.5 us -> none  [body(): lax.all_gather(head_rows, 'tp', axis=1, tiled=True)]
    ppermute x0 -> x15, starting transfers between devices: none -> 40.5 us  [the longest x8 24.8 us: ring_gather(): from_left = lax.ppermute(from_left, axis, ahead)]
    ppermute x0 -> x15, waiting for transfers between devices: none -> 14.9 us  [the longest x8 13.5 us: ring_gather(): from_left = lax.ppermute(from_left, axis, ahead)]
    all_to_all x1, starting transfers between devices: 5.14 us -> 11.9 us  [sent_to_all(): return lax.all_to_all(copies, axis, split_axis=0, concat_axis=0, tiled=True)]
    all_to_all x1, blocking collectives: 27.1 us -> 20.8 us  [body(): lax.all_to_all(outgoing.reshape(senders, rows_most, part_width), SP, spli...]
  transfers between devices with their start and end apart: 9 -> 23, of which waited for: 8 -> 21; matrix products, arithmetic and copies ran while one was open for 2% -> 2% of each run, Pallas kernels for 0% -> 0%
where the time goes in v1:
time: 330 us; the launch traced here: 329 us
  blocking collectives  96.7 us (29%)
  waiting for transfers between devices  96.1 us (29%)
  starting transfers between devices  72.8 us (22%)
  local copies, waits for them, and re-layouts  33.6 us (10%)
  matrix products  15.3 us (5%)
  other arithmetic  13.8 us (4%)
    all_gather x4, blocking collectives, prefix_by_axis(): lax.all_gather(part.astype(kind), axis)  56 us
    ppermute x6, waiting for transfers between devices, from_partner(): return lax.ppermute(value, axis, pairs)  42.8 us
    all_to_all x1, waiting for transfers between devices, sent_to_all(): return lax.all_to_all(copies, axis, split_axis=0, concat_axis=0, tiled=True)  26.5 us
    ppermute x8, starting transfers between devices, ring_gather(): from_left = lax.ppermute(from_left, axis, ahead)  24.8 us
    all_to_all x1, blocking collectives, body(): lax.all_to_all(outgoing.reshape(senders, rows_most, part_width), SP, spli...  20.8 us
    all_gather x1, blocking collectives, body(): lax.all_gather(shared_hidden, 'tp', axis=1, tiled=True)  19.9 us
    ppermute x6, starting transfers between devices, from_partner(): return lax.ppermute(value, axis, pairs)  16.1 us
    ppermute x7, starting transfers between devices, ring_gather(): from_right = lax.ppermute(from_right, axis, left)  15.7 us
  transfers between devices with their start and end apart: 23, of which 21 were waited for; matrix products, arithmetic and copies ran while one was open for 2% of the time, Pallas kernels for 0%

profile of v1, /device:TPU:1, one launch (start us, length us, event | category | flops | bytes accessed | tf_op | source)
XLA Modules:
  0.0 329.2 jit_solution(1025911323187193486)
XLA Ops:
  1.6 1.3 reduce.7
  3.7 1.4 fusion.49
  5.1 1.7 convolution_bitcast_fusion
  7.0 8.5 %all_gather.19 = bf16[4,1,128]{2,1,0:T(2,128)(2,1)S(1)} all-gather(bf16[1,1,128]{2,1,0:T(2,128)(2,1)S(1)} %get-tuple-element.7), channel_id=1, replica_groups=mesh['sp_0'=8,'sp_1'=4,'tp'=16] {'sp_1'}, dimensions={0}, use_global_device_ids=true | all-gather | bytes 1280 | tf_op jit(solution)/shard_map/all_gather | solution.py:52
  15.6 18.6 %all_gather.20 = bf16[8,1,128]{2,1,0:T(2,128)(2,1)S(1)} all-gather(bf16[1,1,128]{2,1,0:T(2,128)(2,1)S(1)} %multiply_convert_fusion.1), channel_id=1, replica_groups=mesh['sp_0'=8,'sp_1'=4,'tp'=16] {'sp_0'}, dimensions={0}, use_global_device_ids=true | all-gather | bytes 2304 | tf_op jit(solution)/shard_map/all_gather | solution.py:52
  34.9 9.4 %all_gather.21 = bf16[4,1,128,256]{3,2,1,0:T(8,128)(2,1)S(1)} all-gather(bf16[1,1,128,256]{3,2,1,0:T(8,128)(2,1)S(1)} %copy.45), channel_id=1, replica_groups=mesh['sp_0'=8,'sp_1'=4,'tp'=16] {'sp_1'}, dimensions={0}, use_global_device_ids=true | all-gather | bytes 327680 | tf_op jit(solution)/shard_map/all_gather | solution.py:52
  44.4 19.5 %all_gather.22 = bf16[8,1,128,256]{3,2,1,0:T(8,128)(2,1)S(1)} all-gather(bf16[1,1,128,256]{3,2,1,0:T(8,128)(2,1)S(1)} %fusion.46), channel_id=1, replica_groups=mesh['sp_0'=8,'sp_1'=4,'tp'=16] {'sp_0'}, dimensions={0}, use_global_device_ids=true | all-gather | bytes 589824 | tf_op jit(solution)/shard_map/all_gather | solution.py:52
  66.4 16.6 %collective-permute-start = (bf16[256,256]{1,0:T(8,128)(2,1)}, bf16[256,256]{1,0:T(8,128)(2,1)S(1)}, u32[]{:S(2)}, u32[]{:S(2)}) collective-permute-start(bf16[256,256]{1,0:T(8,128)(2,1)} %get-tuple-element.26), channel_id=1, source_target_pairs={{0,1},{1,2},{2,3},{3,4},{4,5},{5,6},{6,7},{7,8},{8,9},{9,10},{10,1... | collective-permute-start | bytes 393224 | tf_op jit(solution)/shard_map/ppermute | solution.py:28
  83.0 2.3 collective-permute-done
  85.3 2.3 collective-permute-start.2
  87.7 1.9 collective-permute-done.2
  89.6 2.4 collective-permute-start.4
  94.1 2.3 collective-permute-start.6
  96.7 2.2 collective-permute-start.7
  101.1 3.4 %collective-permute-start.9 = (bf16[256,256]{1,0:T(8,128)(2,1)S(1)}, bf16[256,256]{1,0:T(8,128)(2,1)S(1)}, u32[]{:S(2)}, u32[]{:S(2)}) collective-permute-start(bf16[256,256]{1,0:T(8,128)(2,1)S(1)} %collective-permute-done.7), channel_id=1, source_target_pairs={{0,15},{1,0},{2,1},{3,2},{4,3},{5,4},{6,5},{7,6},{8,7},{9,8},{10,9... | collective-permute-start | bytes 393224 | tf_op jit(solution)/shard_map/ppermute | solution.py:33
  105.5 4.6 %collective-permute-start.11 = (bf16[256,256]{1,0:T(8,128)(2,1)S(1)}, bf16[256,256]{1,0:T(8,128)(2,1)S(1)}, u32[]{:S(2)}, u32[]{:S(2)}) collective-permute-start(bf16[256,256]{1,0:T(8,128)(2,1)S(1)} %collective-permute-done.9), channel_id=1, source_target_pairs={{0,15},{1,0},{2,1},{3,2},{4,3},{5,4},{6,5},{7,6},{8,7},{9,8},{10,9... | collective-permute-start | bytes 393224 | tf_op jit(solution)/shard_map/ppermute | solution.py:33
  111.0 4.6 %collective-permute-start.13 = (bf16[256,256]{1,0:T(8,128)(2,1)S(1)}, bf16[256,256]{1,0:T(8,128)(2,1)S(1)}, u32[]{:S(2)}, u32[]{:S(2)}) collective-permute-start(bf16[256,256]{1,0:T(8,128)(2,1)S(1)} %collective-permute-done.11), channel_id=1, source_target_pairs={{0,15},{1,0},{2,1},{3,2},{4,3},{5,4},{6,5},{7,6},{8,7},{9,8},{10,9... | collective-permute-start | bytes 393224 | tf_op jit(solution)/shard_map/ppermute | solution.py:33
  116.7 5.4 %collective-permute-done.14 = bf16[256,256]{1,0:T(8,128)(2,1)S(1)} collective-permute-done((bf16[256,256]{1,0:T(8,128)(2,1)S(1)}, bf16[256,256]{1,0:T(8,128)(2,1)S(1)}, u32[]{:S(2)}, u32[]{:S(2)}) %collective-permute-start.14) | collective-permute-done | bytes 131104 | tf_op jit(solution)/shard_map/ppermute | solution.py:28
  123.5 1.2 broadcast_in_dim.91
  124.7 11.9 %all-to-all-start = ((bf16[16,256,128]{2,1,0:T(8,128)(2,1)}), bf16[16,256,128]{2,1,0:T(8,128)(2,1)S(1)}, u32[]{:S(2)}, u32[]{:S(2)}) async-start(bf16[16,256,128]{2,1,0:T(8,128)(2,1)} %broadcast_in_dim.91), calls=%async_computation | async-start | bytes 2097152 | tf_op jit(solution)/shard_map/all_to_all | solution.py:75
  138.1 26.5 %all-to-all-done = bf16[16,256,128]{2,1,0:T(8,128)(2,1)S(1)} async-done(((bf16[16,256,128]{2,1,0:T(8,128)(2,1)}), bf16[16,256,128]{2,1,0:T(8,128)(2,1)S(1)}, u32[]{:S(2)}, u32[]{:S(2)}) %all-to-all-start) | async-done | bytes 1048608 | tf_op jit(solution)/shard_map/all_to_all | solution.py:75
  165.2 9.7 %scatter_custom_fusion = bf16[384,512]{1,0:T(8,128)(2,1)S(1)} fusion(s32[1024]{0:T(1024)S(1)} %bitcast.324, bf16[256,512]{1,0:T(8,128)(2,1)S(1)} %constant_dynamic-slice_fusion.2, s32[1024]{0:T(1024)S(1)} %broadcast_clamp_fusion.1, bf16[]{:T(256)} %constant.237.clone.1), kind=kCustom, calls=%fused_computation.26 | custom fusion | bytes 393218 | tf_op jit(solution)/shard_map/scatter | solution.py:226
  175.0 20.8 %all_to_all.15 = bf16[32,12,512]{2,1,0:T(8,128)(2,1)S(1)} all-to-all(bf16[32,12,512]{2,1,0:T(8,128)(2,1)S(1)} %reshape.1386), channel_id=1, replica_groups=mesh['sp_0'=8,'sp_1'=4,'tp'=16] {'sp_0','sp_1'}, dimensions={0} | all-to-all | bytes 786432 | tf_op jit(solution)/shard_map/all_to_all | solution.py:228
  195.8 1.9 collective-permute-start.15
  197.7 1.9 collective-permute-done.15
  200.0 1.3 copy.52
  201.3 2.1 collective-permute-start.16
  204.8 17.7 %collective-permute-done.16 = bf16[32,12,1024]{2,0,1:T(8,128)(2,1)} collective-permute-done((bf16[32,12,1024]{2,0,1:T(8,128)(2,1)}, bf16[32,12,1024]{2,0,1:T(8,128)(2,1)}, u32[]{:S(2)}, u32[]{:S(2)}) %collective-permute-start.16) | collective-permute-done | bytes 786464 | tf_op jit(solution)/shard_map/ppermute | solution.py:85
  222.5 1.6 copy.53
  225.1 2.8 fusion.18
  227.9 5.2 %fusion.19 = f32[384,2048]{1,0:T(8,128)} fusion(bf16[256,2048]{1,0:T(8,128)(2,1)S(1)} %copy-done, f32[384,256]{1,0:T(8,128)S(1)} %fusion.18, bf16[2048,256]{1,0:T(8,128)(2,1)} %param.31, bf16[384,1024]{1,0:T(8,128)(2,1)} %maximum_select_fusion.2, bf16[384,1024]{1,0:T(8,128)(2,1)S(1)} %copy-done.3, pred[]{:T(512)S(6)} %eq.81), kind=kOutput, calls=%fused_computation.48 | convolution fusion | flops 812974080 | bytes 7208961 | tf_op jit(solution)/shard_map/dot_general | solution.py:247
  233.1 5.6 %reshape_reshape.3 = f32[384,4,2,2,128]{4,3,2,1,0:T(2,128)} reshape(f32[384,2048]{1,0:T(8,128)} %fusion.19) | data formatting | bytes 6291456 | tf_op jit(solution)/shard_map/reshape;reshape | solution.py:251
  238.7 1.9 constant_dynamic-slice_fusion
  240.9 2.2 collective-permute-start.17
  243.1 2.0 constant_dynamic-slice_fusion.1
  245.1 15.9 %collective-permute-done.17 = bf16[384,4,2,128]{3,1,0,2:T(4,128)(2,1)} collective-permute-done((bf16[384,4,2,128]{3,1,0,2:T(4,128)(2,1)S(1)}, bf16[384,4,2,128]{3,1,0,2:T(4,128)(2,1)}, u32[]{:S(2)}, u32[]{:S(2)}) %collective-permute-start.17) | collective-permute-done | bytes 786464 | tf_op jit(solution)/shard_map/ppermute | solution.py:85
  261.0 1.7 bitcast_add_fusion
  264.0 3.8 %collective-permute-start.18 = (bf16[384,4,1,128]{3,1,0,2:T(4,128)(2,1)S(1)}, bf16[384,4,1,128]{3,1,0,2:T(4,128)(2,1)S(1)}, u32[]{:S(2)}, u32[]{:S(2)}) collective-permute-start(bf16[384,4,1,128]{3,1,0,2:T(4,128)(2,1)S(1)} %dynamic-slice_convert_fusion), channel_id=1, source_target_pairs={{0,1},{1,0},{2,3},{3,2},{4,5},{5,4},{6,7},{7,6},{8,9},{9,8},{10,11... | collective-permute-start | bytes 1179656 | tf_op jit(solution)/shard_map/ppermute | solution.py:85
  267.8 1.3 collective-permute-done.18
  269.1 2.1 add_convert_fusion
  271.2 4.3 %all-to-all-start.2 = ((bf16[32,12,4,128]{3,2,1,0:T(4,128)(2,1)}), bf16[32,12,4,128]{3,2,1,0:T(4,128)(2,1)S(1)}, u32[]{:S(2)}, u32[]{:S(2)}) async-start(bf16[32,12,4,128]{3,2,1,0:T(4,128)(2,1)} %bitcast.64), calls=%async_computation.2 | async-start | bytes 786432 | tf_op jit(solution)/shard_map/all_to_all | solution.py:262
  277.4 12.0 %all-to-all-done.2 = bf16[32,12,4,128]{3,2,1,0:T(4,128)(2,1)S(1)} async-done(((bf16[32,12,4,128]{3,2,1,0:T(4,128)(2,1)}), bf16[32,12,4,128]{3,2,1,0:T(4,128)(2,1)S(1)}, u32[]{:S(2)}, u32[]{:S(2)}) %all-to-all-start.2) | async-done | bytes 393248 | tf_op jit(solution)/shard_map/all_to_all | solution.py:262
  289.4 3.6 %gather_fusion = bf16[1024,4,128]{2,1,0:T(4,128)(2,1)S(1)} fusion(bf16[384,4,128]{2,1,0:T(4,128)(2,1)S(1)} %bitcast.299, s32[1024]{0:T(1024)S(1)} %broadcast_clamp_fusion), kind=kCustom, calls=%fused_computation.1 | custom fusion | bytes 2101248 | tf_op jit(solution)/shard_map/gather | solution.py:268
  293.0 2.7 fusion.3
  295.9 4.1 %collective-permute-start.19 = (bf16[256,2,128]{2,0,1:T(8,128)(2,1)S(1)}, bf16[256,2,128]{2,0,1:T(8,128)(2,1)S(1)}, u32[]{:S(2)}, u32[]{:S(2)}) collective-permute-start(bf16[256,2,128]{2,0,1:T(8,128)(2,1)S(1)} %fusion.50), channel_id=1, source_target_pairs={{0,8},{1,9},{2,10},{3,11},{4,12},{5,13},{6,14},{7,15},{8,0},{9,1},... | collective-permute-start | bytes 393224 | tf_op jit(solution)/shard_map/ppermute | solution.py:85
  300.5 19.9 %all_gather.23 = bf16[256,512]{0,1:T(8,128)(2,1)S(1)} all-gather(bf16[256,32]{0,1:T(8,128)(2,1)S(1)} %fusion.7), channel_id=1, replica_groups=mesh['sp_0'=8,'sp_1'=4,'tp'=16] {'tp'}, dimensions={1}, use_global_device_ids=true | all-gather | bytes 278528 | tf_op jit(solution)/shard_map/all_gather | solution.py:258
  320.4 1.9 collective-permute-start.20
  322.6 6.0 %collective-permute-done.20 = bf16[256,1,128]{2,0,1:T(8,128)(2,1)S(1)} collective-permute-done((bf16[256,1,128]{2,0,1:T(8,128)(2,1)S(1)}, bf16[256,1,128]{2,0,1:T(8,128)(2,1)S(1)}, u32[]{:S(2)}, u32[]{:S(2)}) %collective-permute-start.20) | collective-permute-done | bytes 65568 | tf_op jit(solution)/shard_map/ppermute | solution.py:85
  (148 shorter events, 24.4 us)
Async XLA Ops:
  0.0 227.9 %copy-start = (bf16[256,2048]{1,0:T(8,128)(2,1)S(1)}, bf16[256,2048]{1,0:T(8,128)(2,1)}, u32[]{:S(2)}) copy-start(bf16[256,2048]{1,0:T(8,128)(2,1)} %param.32) | copy-start | bytes 3145732
  3.3 30.8 %copy-start.18 = (bf16[256]{0:T(256)(128)(2,1)S(1)}, bf16[256]{0:T(256)(128)(2,1)}, u32[]{:S(2)}) copy-start(bf16[256]{0:T(256)(128)(2,1)} %param.24) | copy-start | bytes 1540
  3.3 30.9 %copy-start.13 = (bf16[256,128]{1,0:T(8,128)(2,1)S(1)}, bf16[256,128]{1,0:T(8,128)(2,1)}, u32[]{:S(2)}) copy-start(bf16[256,128]{1,0:T(8,128)(2,1)} %param.18) | copy-start | bytes 196612
  3.7 30.6 %copy-start.7 = (bf16[256,128]{1,0:T(8,128)(2,1)S(1)}, bf16[256,128]{1,0:T(8,128)(2,1)}, u32[]{:S(2)}) copy-start(bf16[256,128]{1,0:T(8,128)(2,1)} %param.19) | copy-start | bytes 196612
  5.1 29.5 %copy-start.6 = (bf16[256,256]{1,0:T(8,128)(2,1)S(1)}, bf16[256,256]{1,0:T(8,128)(2,1)}, u32[]{:S(2)}) copy-start(bf16[256,256]{1,0:T(8,128)(2,1)} %param.20) | copy-start | bytes 393220
  64.4 1.1 copy-start.11
  66.4 18.9 %collective-permute-start = (bf16[256,256]{1,0:T(8,128)(2,1)}, bf16[256,256]{1,0:T(8,128)(2,1)S(1)}, u32[]{:S(2)}, u32[]{:S(2)}) collective-permute-start(bf16[256,256]{1,0:T(8,128)(2,1)} %get-tuple-element.26), channel_id=1, source_target_pairs={{0,1},{1,2},{2,3},{3,4},{4,5},{5,6},{6,7},{7,8},{8,9},{9,10},{10,1... | collective-permute-start | bytes 393224 | tf_op jit(solution)/shard_map/ppermute | solution.py:28
  83.0 4.6 %collective-permute-start.1 = (bf16[256,256]{1,0:T(8,128)(2,1)}, bf16[256,256]{1,0:T(8,128)(2,1)S(1)}, u32[]{:S(2)}, u32[]{:S(2)}) collective-permute-start(bf16[256,256]{1,0:T(8,128)(2,1)} %get-tuple-element.26), channel_id=1, source_target_pairs={{0,15},{1,0},{2,1},{3,2},{4,3},{5,4},{6,5},{7,6},{8,7},{9,8},{10,9... | collective-permute-start | bytes 393224 | tf_op jit(solution)/shard_map/ppermute | solution.py:33
  83.0 39.1 %copy-start.14 = (bf16[256,128]{1,0:T(8,128)(2,1)S(1)}, bf16[256,128]{1,0:T(8,128)(2,1)}, u32[]{:S(2)}) copy-start(bf16[256,128]{1,0:T(8,128)(2,1)} %param.26) | copy-start | bytes 196612
  83.0 39.1 %copy-start.2 = (bf16[4096,128]{1,0:T(8,128)(2,1)S(1)}, bf16[4096,128]{1,0:T(8,128)(2,1)}, u32[]{:S(2)}) copy-start(bf16[4096,128]{1,0:T(8,128)(2,1)} %param.25) | copy-start | bytes 3145732
  85.3 4.3 %collective-permute-start.2 = (bf16[256,256]{1,0:T(8,128)(2,1)S(1)}, bf16[256,256]{1,0:T(8,128)(2,1)S(1)}, u32[]{:S(2)}, u32[]{:S(2)}) collective-permute-start(bf16[256,256]{1,0:T(8,128)(2,1)S(1)} %collective-permute-done), channel_id=1, source_target_pairs={{0,1},{1,2},{2,3},{3,4},{4,5},{5,6},{6,7},{7,8},{8,9},{9,10},{10,1... | collective-permute-start | bytes 393224 | tf_op jit(solution)/shard_map/ppermute | solution.py:28
  87.6 4.7 %collective-permute-start.3 = (bf16[256,256]{1,0:T(8,128)(2,1)S(1)}, bf16[256,256]{1,0:T(8,128)(2,1)S(1)}, u32[]{:S(2)}, u32[]{:S(2)}) collective-permute-start(bf16[256,256]{1,0:T(8,128)(2,1)S(1)} %collective-permute-done.1), channel_id=1, source_target_pairs={{0,15},{1,0},{2,1},{3,2},{4,3},{5,4},{6,5},{7,6},{8,7},{9,8},{10,9... | collective-permute-start | bytes 393224 | tf_op jit(solution)/shard_map/ppermute | solution.py:33
  89.6 4.5 %collective-permute-start.4 = (bf16[256,256]{1,0:T(8,128)(2,1)S(1)}, bf16[256,256]{1,0:T(8,128)(2,1)S(1)}, u32[]{:S(2)}, u32[]{:S(2)}) collective-permute-start(bf16[256,256]{1,0:T(8,128)(2,1)S(1)} %collective-permute-done.2), channel_id=1, source_target_pairs={{0,1},{1,2},{2,3},{3,4},{4,5},{5,6},{6,7},{7,8},{8,9},{9,10},{10,1... | collective-permute-start | bytes 393224 | tf_op jit(solution)/shard_map/ppermute | solution.py:28
  92.3 4.4 %collective-permute-start.5 = (bf16[256,256]{1,0:T(8,128)(2,1)S(1)}, bf16[256,256]{1,0:T(8,128)(2,1)S(1)}, u32[]{:S(2)}, u32[]{:S(2)}) collective-permute-start(bf16[256,256]{1,0:T(8,128)(2,1)S(1)} %collective-permute-done.3), channel_id=1, source_target_pairs={{0,15},{1,0},{2,1},{3,2},{4,3},{5,4},{6,5},{7,6},{8,7},{9,8},{10,9... | collective-permute-start | bytes 393224 | tf_op jit(solution)/shard_map/ppermute | solution.py:33
  94.1 5.6 %collective-permute-start.6 = (bf16[256,256]{1,0:T(8,128)(2,1)S(1)}, bf16[256,256]{1,0:T(8,128)(2,1)S(1)}, u32[]{:S(2)}, u32[]{:S(2)}) collective-permute-start(bf16[256,256]{1,0:T(8,128)(2,1)S(1)} %collective-permute-done.4), channel_id=1, source_target_pairs={{0,1},{1,2},{2,3},{3,4},{4,5},{5,6},{6,7},{7,8},{8,9},{9,10},{10,1... | collective-permute-start | bytes 393224 | tf_op jit(solution)/shard_map/ppermute | solution.py:28
  96.7 4.4 %collective-permute-start.7 = (bf16[256,256]{1,0:T(8,128)(2,1)S(1)}, bf16[256,256]{1,0:T(8,128)(2,1)S(1)}, u32[]{:S(2)}, u32[]{:S(2)}) collective-permute-start(bf16[256,256]{1,0:T(8,128)(2,1)S(1)} %collective-permute-done.5), channel_id=1, source_target_pairs={{0,15},{1,0},{2,1},{3,2},{4,3},{5,4},{6,5},{7,6},{8,7},{9,8},{10,9... | collective-permute-start | bytes 393224 | tf_op jit(solution)/shard_map/ppermute | solution.py:33
  99.7 5.6 %collective-permute-start.8 = (bf16[256,256]{1,0:T(8,128)(2,1)S(1)}, bf16[256,256]{1,0:T(8,128)(2,1)S(1)}, u32[]{:S(2)}, u32[]{:S(2)}) collective-permute-start(bf16[256,256]{1,0:T(8,128)(2,1)S(1)} %collective-permute-done.6), channel_id=1, source_target_pairs={{0,1},{1,2},{2,3},{3,4},{4,5},{5,6},{6,7},{7,8},{8,9},{9,10},{10,1... | collective-permute-start | bytes 393224 | tf_op jit(solution)/shard_map/ppermute | solution.py:28
  101.1 4.4 %collective-permute-start.9 = (bf16[256,256]{1,0:T(8,128)(2,1)S(1)}, bf16[256,256]{1,0:T(8,128)(2,1)S(1)}, u32[]{:S(2)}, u32[]{:S(2)}) collective-permute-start(bf16[256,256]{1,0:T(8,128)(2,1)S(1)} %collective-permute-done.7), channel_id=1, source_target_pairs={{0,15},{1,0},{2,1},{3,2},{4,3},{5,4},{6,5},{7,6},{8,7},{9,8},{10,9... | collective-permute-start | bytes 393224 | tf_op jit(solution)/shard_map/ppermute | solution.py:33
  105.3 5.6 %collective-permute-start.10 = (bf16[256,256]{1,0:T(8,128)(2,1)S(1)}, bf16[256,256]{1,0:T(8,128)(2,1)S(1)}, u32[]{:S(2)}, u32[]{:S(2)}) collective-permute-start(bf16[256,256]{1,0:T(8,128)(2,1)S(1)} %collective-permute-done.8), channel_id=1, source_target_pairs={{0,1},{1,2},{2,3},{3,4},{4,5},{5,6},{6,7},{7,8},{8,9},{9,10},{10,1... | collective-permute-start | bytes 393224 | tf_op jit(solution)/shard_map/ppermute | solution.py:28
  105.5 5.6 %collective-permute-start.11 = (bf16[256,256]{1,0:T(8,128)(2,1)S(1)}, bf16[256,256]{1,0:T(8,128)(2,1)S(1)}, u32[]{:S(2)}, u32[]{:S(2)}) collective-permute-start(bf16[256,256]{1,0:T(8,128)(2,1)S(1)} %collective-permute-done.9), channel_id=1, source_target_pairs={{0,15},{1,0},{2,1},{3,2},{4,3},{5,4},{6,5},{7,6},{8,7},{9,8},{10,9... | collective-permute-start | bytes 393224 | tf_op jit(solution)/shard_map/ppermute | solution.py:33
  110.9 5.6 %collective-permute-start.12 = (bf16[256,256]{1,0:T(8,128)(2,1)S(1)}, bf16[256,256]{1,0:T(8,128)(2,1)S(1)}, u32[]{:S(2)}, u32[]{:S(2)}) collective-permute-start(bf16[256,256]{1,0:T(8,128)(2,1)S(1)} %collective-permute-done.10), channel_id=1, source_target_pairs={{0,1},{1,2},{2,3},{3,4},{4,5},{5,6},{6,7},{7,8},{8,9},{9,10},{10,1... | collective-permute-start | bytes 393224 | tf_op jit(solution)/shard_map/ppermute | solution.py:28
  111.0 5.6 %collective-permute-start.13 = (bf16[256,256]{1,0:T(8,128)(2,1)S(1)}, bf16[256,256]{1,0:T(8,128)(2,1)S(1)}, u32[]{:S(2)}, u32[]{:S(2)}) collective-permute-start(bf16[256,256]{1,0:T(8,128)(2,1)S(1)} %collective-permute-done.11), channel_id=1, source_target_pairs={{0,15},{1,0},{2,1},{3,2},{4,3},{5,4},{6,5},{7,6},{8,7},{9,8},{10,9... | collective-permute-start | bytes 393224 | tf_op jit(solution)/shard_map/ppermute | solution.py:33
  116.5 5.6 %collective-permute-start.14 = (bf16[256,256]{1,0:T(8,128)(2,1)S(1)}, bf16[256,256]{1,0:T(8,128)(2,1)S(1)}, u32[]{:S(2)}, u32[]{:S(2)}) collective-permute-start(bf16[256,256]{1,0:T(8,128)(2,1)S(1)} %collective-permute-done.12), channel_id=1, source_target_pairs={{0,1},{1,2},{2,3},{3,4},{4,5},{5,6},{6,7},{7,8},{8,9},{9,10},{10,1... | collective-permute-start | bytes 393224 | tf_op jit(solution)/shard_map/ppermute | solution.py:28
  122.8 0.6 copy-start.4
  123.5 13.1 %copy-start.15 = (s32[256,4]{0,1:T(4,128)S(1)}, s32[256,4]{0,1:T(4,128)}, u32[]{:S(2)}) copy-start(s32[256,4]{0,1:T(4,128)} %param.28) | copy-start | bytes 12292
  123.5 13.6 %copy-start.17 = (bf16[2048]{0:T(1024)(128)(2,1)S(1)}, bf16[2048]{0:T(1024)(128)(2,1)}, u32[]{:S(2)}) copy-start(bf16[2048]{0:T(1024)(128)(2,1)} %param.27) | copy-start | bytes 12292
  124.7 39.9 %all-to-all-start = ((bf16[16,256,128]{2,1,0:T(8,128)(2,1)}), bf16[16,256,128]{2,1,0:T(8,128)(2,1)S(1)}, u32[]{:S(2)}, u32[]{:S(2)}) async-start(bf16[16,256,128]{2,1,0:T(8,128)(2,1)} %broadcast_in_dim.91), calls=%async_computation | async-start | bytes 2097152 | tf_op jit(solution)/shard_map/all_to_all | solution.py:75
  195.8 3.8 %collective-permute-start.15 = (bf16[32,12,512]{2,1,0:T(8,128)(2,1)S(1)}, bf16[32,12,512]{2,1,0:T(8,128)(2,1)S(1)}, u32[]{:S(2)}, u32[]{:S(2)}) collective-permute-start(bf16[32,12,512]{2,1,0:T(8,128)(2,1)S(1)} %all_to_all.15), channel_id=1, source_target_pairs={{0,1},{1,0},{2,3},{3,2},{4,5},{5,4},{6,7},{7,6},{8,9},{9,8},{10,11... | collective-permute-start | bytes 1179656 | tf_op jit(solution)/shard_map/ppermute | solution.py:85
  201.3 21.2 %collective-permute-start.16 = (bf16[32,12,1024]{2,0,1:T(8,128)(2,1)}, bf16[32,12,1024]{2,0,1:T(8,128)(2,1)}, u32[]{:S(2)}, u32[]{:S(2)}) collective-permute-start(bf16[32,12,1024]{2,0,1:T(8,128)(2,1)} %copy.52), channel_id=1, source_target_pairs={{0,2},{1,3},{2,0},{3,1},{4,6},{5,7},{6,4},{7,5},{8,10},{9,11},{10,... | collective-permute-start | bytes 2359304 | tf_op jit(solution)/shard_map/ppermute | solution.py:85
  225.1 2.8 copy-start.3
  240.9 20.1 %collective-permute-start.17 = (bf16[384,4,2,128]{3,1,0,2:T(4,128)(2,1)S(1)}, bf16[384,4,2,128]{3,1,0,2:T(4,128)(2,1)}, u32[]{:S(2)}, u32[]{:S(2)}) collective-permute-start(bf16[384,4,2,128]{3,1,0,2:T(4,128)(2,1)S(1)} %bitcast.308), channel_id=1, source_target_pairs={{0,2},{1,3},{2,0},{3,1},{4,6},{5,7},{6,4},{7,5},{8,10},{9,11},{10,... | collective-permute-start | bytes 2359304 | tf_op jit(solution)/shard_map/ppermute | solution.py:85
  262.7 1.2 copy-start.1
  263.9 11.7 %copy-start.16 = (f32[256,4]{0,1:T(4,128)S(1)}, f32[256,4]{0,1:T(4,128)}, u32[]{:S(2)}) copy-start(f32[256,4]{0,1:T(4,128)} %param.29) | copy-start | bytes 12292
  263.9 12.5 %copy-start.8 = (bf16[2048,32]{0,1:T(8,128)(2,1)S(1)}, bf16[2048,32]{0,1:T(8,128)(2,1)}, u32[]{:S(2)}) copy-start(bf16[2048,32]{0,1:T(8,128)(2,1)} %param.33) | copy-start | bytes 393220
  264.0 5.1 %collective-permute-start.18 = (bf16[384,4,1,128]{3,1,0,2:T(4,128)(2,1)S(1)}, bf16[384,4,1,128]{3,1,0,2:T(4,128)(2,1)S(1)}, u32[]{:S(2)}, u32[]{:S(2)}) collective-permute-start(bf16[384,4,1,128]{3,1,0,2:T(4,128)(2,1)S(1)} %dynamic-slice_convert_fusion), channel_id=1, source_target_pairs={{0,1},{1,0},{2,3},{3,2},{4,5},{5,4},{6,7},{7,6},{8,9},{9,8},{10,11... | collective-permute-start | bytes 1179656 | tf_op jit(solution)/shard_map/ppermute | solution.py:85
  271.2 18.2 %all-to-all-start.2 = ((bf16[32,12,4,128]{3,2,1,0:T(4,128)(2,1)}), bf16[32,12,4,128]{3,2,1,0:T(4,128)(2,1)S(1)}, u32[]{:S(2)}, u32[]{:S(2)}) async-start(bf16[32,12,4,128]{3,2,1,0:T(4,128)(2,1)} %bitcast.64), calls=%async_computation.2 | async-start | bytes 786432 | tf_op jit(solution)/shard_map/all_to_all | solution.py:262
  293.0 7.0 %copy-start.9 = (bf16[2048,32]{0,1:T(8,128)(2,1)S(1)}, bf16[2048,32]{0,1:T(8,128)(2,1)}, u32[]{:S(2)}) copy-start(bf16[2048,32]{0,1:T(8,128)(2,1)} %param.34) | copy-start | bytes 393220
  293.0 7.0 %copy-start.10 = (f32[256,32]{0,1:T(8,128)S(1)}, f32[256,32]{0,1:T(8,128)}, u32[]{:S(2)}) copy-start(f32[256,32]{0,1:T(8,128)} %fusion.143) | copy-start | bytes 98308
  295.8 26.6 %copy-start.12 = (bf16[512,128]{1,0:T(8,128)(2,1)S(1)}, bf16[512,128]{1,0:T(8,128)(2,1)}, u32[]{:S(2)}) copy-start(bf16[512,128]{1,0:T(8,128)(2,1)} %param.35) | copy-start | bytes 393220
  295.8 32.8 %copy-start.5 = (bf16[256,128]{1,0:T(8,128)(2,1)S(1)}, bf16[256,128]{1,0:T(8,128)(2,1)}, u32[]{:S(2)}) copy-start(bf16[256,128]{1,0:T(8,128)(2,1)} %copy-done.4) | copy-start | bytes 196612
  295.9 24.5 %collective-permute-start.19 = (bf16[256,2,128]{2,0,1:T(8,128)(2,1)S(1)}, bf16[256,2,128]{2,0,1:T(8,128)(2,1)S(1)}, u32[]{:S(2)}, u32[]{:S(2)}) collective-permute-start(bf16[256,2,128]{2,0,1:T(8,128)(2,1)S(1)} %fusion.50), channel_id=1, source_target_pairs={{0,8},{1,9},{2,10},{3,11},{4,12},{5,13},{6,14},{7,15},{8,0},{9,1},... | collective-permute-start | bytes 393224 | tf_op jit(solution)/shard_map/ppermute | solution.py:85
  320.4 8.2 %collective-permute-start.20 = (bf16[256,1,128]{2,0,1:T(8,128)(2,1)S(1)}, bf16[256,1,128]{2,0,1:T(8,128)(2,1)S(1)}, u32[]{:S(2)}, u32[]{:S(2)}) collective-permute-start(bf16[256,1,128]{2,0,1:T(8,128)(2,1)S(1)} %dynamic-slice_convert_fusion.2), channel_id=1, source_target_pairs={{0,4},{1,5},{2,6},{3,7},{4,0},{5,1},{6,2},{7,3},{8,12},{9,13},{10,... | collective-permute-start | bytes 196616 | tf_op jit(solution)/shard_map/ppermute | solution.py:85
